TPU v7x, 32 devices: a whole 2x2x4 slice. The times are simulated.
32 devices in a mesh: fs: 8 (over z, x), tp: 4 (over y, core).
Axes of the slice: x: 2, y: 2, z: 4, core: 2. Of those that a mesh axis runs over, the one named last changes fastest.
Arguments:
- late_input: bfloat16 [4096, 2048], P(('fs', 'tp')), may hold values from -6 to 6
- norm_gain: bfloat16 [2048], replicated, may hold values from 0.099609375 to 1.8984375
- gate_weight: bfloat16 [2048, 2816], P('fs', 'tp'), may hold values from -0.125 to 0.125
- up_weight: bfloat16 [2048, 2816], P('fs', 'tp'), may hold values from -0.125 to 0.125
- down_weight: bfloat16 [2048, 2816], P('fs', 'tp'), may hold values from -0.109375 to 0.109375
- early_input: bfloat16 [4096, 2048], P(('fs', 'tp')), may hold values from -6 to 6
- cotangent: bfloat16 [4096, 2048], P(('fs', 'tp')), may hold values from -6 to 6
- gate_sum: float32 [2048, 2816], P('fs', 'tp'), may hold values from -192 to 192
- up_sum: float32 [2048, 2816], P('fs', 'tp'), may hold values from -192 to 192
- down_sum: float32 [2048, 2816], P('fs', 'tp'), may hold values from -192 to 192
- gain_sum: float32 [2048], replicated, may hold values from -192 to 192
Outputs:
- late_out: bfloat16 [4096, 2048], P(('fs', 'tp'))
- early_grad: bfloat16 [4096, 2048], P(('fs', 'tp'))
- gate_sum_out: float32 [2048, 2816], P('fs', 'tp')
- up_sum_out: float32 [2048, 2816], P('fs', 'tp')
- down_sum_out: float32 [2048, 2816], P('fs', 'tp')
- gain_sum_out: float32 [2048], replicated
All inputs are finite; a program needn't handle non-finite values.
Results may differ from a plain program's by a relative error of at most 0.008.
Values may be sent and summed in bfloat16 or wider, within the bound.
A program may use at most 128 MiB of HBM per device.

v0:
```python
import functools

import jax
import jax.numpy as jnp
from jax import lax
from jax.experimental import pallas as pl
from jax.experimental.pallas import tpu as pltpu
from jax.sharding import PartitionSpec as P

epsilon = 1e-05
MESH = pl.DeviceIdType.MESH
VMEM_LIMIT = 60 * 1024 * 1024


def ring_place(index, n):
    odd = lax.rem(index, 2)
    half = index // 2
    return (1 - odd) * half + odd * (n - 1 - half)


def ring_index(place, n):
    back = place // (n // 2)
    return (1 - back) * (2 * place) + back * (2 * (n - 1 - place) + 1)


def neighbours(n):
    place = ring_place(lax.axis_index("fs"), n)
    right = ring_index(lax.rem(place + 1, n), n)
    left = ring_index(lax.rem(place + n - 1, n), n)
    return place, right, left


def greet(n_tp, right, left):
    me_tp = lax.axis_index("tp")
    barrier = pltpu.get_barrier_semaphore()
    for target in (right, left):
        pl.semaphore_signal(barrier, inc=1, device_id=(target, me_tp), device_id_type=MESH)
    for away in range(1, n_tp):
        peer = lax.rem(me_tp + away, n_tp)
        pl.semaphore_signal(
            barrier, inc=1, device_id=(lax.axis_index("fs"), peer), device_id_type=MESH
        )
    pl.semaphore_wait(barrier, 2 + n_tp - 1)


def gather_kernel(n, n_tp, turned, *refs):
    gate_in, up_in, dn_in, late_in, early_in, cot_ref, gain_ref = refs[:7]
    gu_out, dn_out, late_all, early_out, cot_out, both_out, hid_out = refs[7:14]
    gate_buf, up_buf, gu_ref, dn_buf, dn_ref, late_buf, early_buf, late_ref = refs[14:22]
    gu_all, dn_all, early_all, cot_all, sum_gu, sum_dn = refs[22:28]
    send_sem, recv_sem, tp_send, tp_recv, own_sem, in_sem, out_sem = refs[28:]
    me_fs, me_tp = lax.axis_index("fs"), lax.axis_index("tp")
    tokens = late_in.shape[0]
    mine = pl.ds(pl.multiple_of(me_tp * tokens, tokens), tokens)
    rows, width = dn_ref.shape
    loads = [
        pltpu.make_async_copy(source, target, in_sem.at[k])
        for k, (source, target) in enumerate(
            (
                (gate_in, gate_buf),
                (up_in, up_buf),
                (early_in, early_buf),
                (late_in, late_buf),
                (dn_in, dn_buf),
                (cot_ref, cot_all.at[mine]),
            )
        )
    ]
    for copy in loads:
        copy.start()
    place, right, left = neighbours(n)
    greet(n_tp, right, left)
    half = rows // 2
    outs = (gu_out, dn_out)
    pairs = ((gu_ref, gu_all), (dn_ref, dn_all))

    def window(owner, way):
        return pl.ds(pl.multiple_of(owner * rows + way * half, half), half)

    def piece(step, c, way, first):
        block, whole = pairs[c]
        if way == 0:
            owner = ring_index(lax.rem(place - step + n, n), n)
            target = right
        else:
            owner = ring_index(lax.rem(place + step, n), n)
            target = left
        spot = whole.at[window(owner, way)]
        source = block.at[pl.ds(way * half, half)] if first else spot
        return pltpu.make_async_remote_copy(
            src_ref=source,
            dst_ref=spot,
            send_sem=send_sem.at[step, c, way],
            recv_sem=recv_sem.at[step, c, way],
            device_id=(target, me_tp),
            device_id_type=MESH,
        )

    token_pairs = (
        (early_all.at[mine], early_all),
        (cot_ref, cot_all),
        (late_ref, late_all),
    )

    def token_piece(a, away):
        block, whole = token_pairs[a]
        return pltpu.make_async_remote_copy(
            src_ref=block,
            dst_ref=whole.at[mine],
            send_sem=tp_send.at[a, away - 1],
            recv_sem=tp_recv.at[a, away - 1],
            device_id=(me_fs, lax.rem(me_tp + away, n_tp)),
            device_id_type=MESH,
        )

    def spread(a):
        for away in range(1, n_tp):
            token_piece(a, away).start()

    def arrived(a):
        for away in range(1, n_tp):
            token_piece(a, away).wait()

    def owner_of(step, way):
        if way == 0:
            return ring_index(lax.rem(place - step + n, n), n)
        return ring_index(lax.rem(place + step, n), n)

    def landed(step, c, way):
        some = window(owner_of(step + 1, way), way)
        return pltpu.make_async_copy(
            pairs[c][1].at[some], outs[c].at[some], out_sem.at[step, c, way]
        )

    totals = ((sum_gu, early_all), (sum_dn, cot_all))

    def add_rows(step, c):
        total, left = totals[c]
        for way in range(2):
            some = window(owner_of(step, way), way)
            total[...] += jnp.dot(
                left[:, some], pairs[c][1][some, :], preferred_element_type=jnp.float32
            )

    def norm(source, target, base):
        def part(k, carry):
            some = pl.ds(pl.multiple_of(k * 16, 16), 16)
            values = source[some, :].astype(jnp.float32)
            scale = lax.rsqrt(jnp.mean(values * values, axis=-1, keepdims=True) + epsilon)
            target[pl.ds(pl.multiple_of(base + k * 16, 16), 16), :] = (values * scale * gain_ref[...]).astype(jnp.bfloat16)
            return carry

        lax.fori_loop(0, tokens // 16, part, 0)

    def plain(buffer):
        return buffer[...].T if turned else buffer[...]

    loads[4].wait()
    dn_ref[...] = plain(dn_buf)
    for way in range(2):
        piece(0, 1, way, True).start()
    loads[0].wait()
    loads[1].wait()
    gu_ref[:, :width] = plain(gate_buf)
    gu_ref[:, width:] = plain(up_buf)
    for way in range(2):
        piece(0, 0, way, True).start()
    loads[2].wait()
    norm(early_buf, early_all, me_tp * tokens)
    spread(0)
    spread(1)
    loads[3].wait()
    norm(late_buf, late_ref, 0)
    spread(2)
    loads[5].wait()
    here = pl.ds(pl.multiple_of(me_fs * rows, rows), rows)
    gu_all[here, :] = gu_ref[...]
    dn_all[here, :] = dn_ref[...]
    sum_gu[...] = jnp.zeros_like(sum_gu)
    sum_dn[...] = jnp.zeros_like(sum_dn)
    own = [
        pltpu.make_async_copy(late_ref, late_all.at[mine], own_sem.at[0]),
        pltpu.make_async_copy(gu_ref, gu_out.at[here], own_sem.at[1]),
        pltpu.make_async_copy(dn_ref, dn_out.at[here], own_sem.at[2]),
    ]
    for copy in own:
        copy.start()
    keep = [
        pltpu.make_async_copy(early_all, early_out, own_sem.at[3]),
        pltpu.make_async_copy(cot_all, cot_out, own_sem.at[4]),
    ]

    def body(step, carry):
        for c in (1, 0):
            for way in range(2):
                piece(step - 1, c, way, False).wait_recv()
                piece(step, c, way, False).start()
                landed(step - 1, c, way).start()
            which = 1 - c

            @pl.when(step == n // 2)
            def _():
                arrived(which)
                keep[which].start()

            if turned:

                @pl.when(step >= n // 2)
                def _():
                    add_rows(2 * (step - n // 2), which)
                    add_rows(2 * (step - n // 2) + 1, which)

        return carry

    lax.fori_loop(1, n - 1, body, 0)
    if turned:
        for c in (1, 0):
            add_rows(n - 2, c)
    for c in (1, 0):
        for way in range(2):
            piece(n - 2, c, way, False).wait_recv()
            landed(n - 2, c, way).start()
            piece(0, c, way, True).wait_send()
        if turned:
            add_rows(n - 1, c)
        else:
            total, rest = totals[c]
            total[...] = jnp.dot(
                rest[...], pairs[c][1][...], preferred_element_type=jnp.float32
            )

    def finish(k, carry):
        some = pl.ds(pl.multiple_of(k * 64, 64), 64)
        gate, upper = sum_gu[some, :width], sum_gu[some, width:]
        sigma = 1.0 / (1.0 + jnp.exp(-gate))
        d_hidden = 0.5 * sum_dn[some, :]
        hid_out[some, :] = (gate * sigma * upper).astype(jnp.bfloat16)
        both_out[some, :width] = (
            d_hidden * upper * sigma * (1.0 + gate * (1.0 - sigma))
        ).astype(jnp.bfloat16)
        both_out[some, width:] = (d_hidden * gate * sigma).astype(jnp.bfloat16)
        return carry

    lax.fori_loop(0, n_tp * tokens // 64, finish, 0)

    def drain(step, carry):
        for c in (1, 0):
            for way in range(2):
                piece(step, c, way, False).wait_send()
        return carry

    lax.fori_loop(1, n - 1, drain, 0)

    def put(step, carry):
        for c in range(2):
            for way in range(2):
                landed(step, c, way).wait()
        return carry

    lax.fori_loop(0, n - 1, put, 0)
    for copy in own + keep:
        copy.wait()
    arrived(2)


def gather(n, n_tp, turned, gate, up, dn, late, early, cot, gain):
    rows, width = gate.shape[::-1] if turned else gate.shape
    tokens, depth = late.shape
    vmem = pl.BlockSpec(memory_space=pltpu.VMEM)
    hbm = pl.BlockSpec(memory_space=pl.ANY)
    bf16 = jnp.bfloat16
    return pl.pallas_call(
        functools.partial(gather_kernel, n, n_tp, turned),
        out_shape=[
            jax.ShapeDtypeStruct((n * rows, 2 * width), bf16),
            jax.ShapeDtypeStruct((n * rows, width), bf16),
        ]
        + [jax.ShapeDtypeStruct((n_tp * tokens, depth), bf16)] * 3
        + [
            jax.ShapeDtypeStruct((n_tp * tokens, 2 * width), bf16),
            jax.ShapeDtypeStruct((n_tp * tokens, width), bf16),
        ],
        in_specs=[hbm] * 6 + [vmem],
        out_specs=[hbm] * 5 + [vmem] * 2,
        scratch_shapes=[
            pltpu.VMEM(gate.shape, bf16),
            pltpu.VMEM(gate.shape, bf16),
            pltpu.VMEM((rows, 2 * width), bf16),
            pltpu.VMEM(gate.shape, bf16),
            pltpu.VMEM((rows, width), bf16),
        ]
        + [pltpu.VMEM((tokens, depth), bf16)] * 3
        + [
            pltpu.VMEM((n * rows, 2 * width), bf16),
            pltpu.VMEM((n * rows, width), bf16),
            pltpu.VMEM((n_tp * tokens, depth), bf16),
            pltpu.VMEM((n_tp * tokens, depth), bf16),
            pltpu.VMEM((n_tp * tokens, 2 * width), jnp.float32),
            pltpu.VMEM((n_tp * tokens, width), jnp.float32),
        ]
        + [
            pltpu.SemaphoreType.DMA((n - 1, 2, 2)),
            pltpu.SemaphoreType.DMA((n - 1, 2, 2)),
            pltpu.SemaphoreType.DMA((3, n_tp - 1)),
            pltpu.SemaphoreType.DMA((3, n_tp - 1)),
            pltpu.SemaphoreType.DMA((5,)),
            pltpu.SemaphoreType.DMA((6,)),
            pltpu.SemaphoreType.DMA((n - 1, 2, 2)),
        ],
        compiler_params=pltpu.CompilerParams(
            collective_id=0, has_side_effects=True, vmem_limit_bytes=VMEM_LIMIT
        ),
    )(gate, up, dn, late, early, cot, gain)


def reduce_kernel(n, n_tp, turned, *refs):
    early_side, cot_side, both_ref, hid_ref, gain_ref, early_all, gu_in, dn_in, late_in = refs[:9]
    gu_out, dn_out, mix_out, dnorm_out, gain_out = refs[9:14]
    gu_slots, dn_slots, gain_slots, gain_tp, gu_first, dn_first = refs[14:20]
    gu_all, dn_all, late_all, mix_ref, dnorm_ref, gain_sum = refs[20:26]
    send_sem, recv_sem, gain_send, gain_recv, tp_send, tp_recv, last_send, last_recv = refs[26:34]
    in_sem, own_sem = refs[34:]
    loads = [
        pltpu.make_async_copy(source, target, in_sem.at[k])
        for k, (source, target) in enumerate(
            ((gu_in, gu_all), (late_in, late_all), (dn_in, dn_all))
        )
    ]
    for copy in loads:
        copy.start()
    me_fs, me_tp = lax.axis_index("fs"), lax.axis_index("tp")
    place, right, left = neighbours(n)
    barrier = pltpu.get_barrier_semaphore()

    def greet_fs(away, carry):
        target = lax.rem(me_fs + away, n)
        pl.semaphore_signal(barrier, inc=1, device_id=(target, me_tp), device_id_type=MESH)
        return carry

    lax.fori_loop(1, n, greet_fs, 0)
    for away in range(1, n_tp):
        peer = lax.rem(me_tp + away, n_tp)
        pl.semaphore_signal(barrier, inc=1, device_id=(me_fs, peer), device_id_type=MESH)
    pl.semaphore_wait(barrier, n - 1 + n_tp - 1)
    width = dn_all.shape[1]
    half = gu_first.shape[1]
    rows = 2 * half
    tokens = late_all.shape[0] // n_tp
    sets = ((gu_first, gu_slots), (dn_first, dn_slots))
    factors = ((early_side, both_ref, 1.0), (cot_side, hid_ref, 0.5))

    def local(step, way):
        if way == 0:
            owner = ring_index(lax.rem(place - step - 1 + n, n), n)
        else:
            owner = ring_index(lax.rem(place + step + 1, n), n)
        return pl.ds(pl.multiple_of(owner * rows + way * half, half), half)

    def product(step, c, way):
        side, other, factor = factors[c]
        if turned:
            left, contract = side[:, local(step, way)], 0
        else:
            left, contract = side[local(step, way), :], 1
        return factor * lax.dot_general(
            left,
            other[...],
            (((contract,), (0,)), ((), ())),
            preferred_element_type=jnp.float32,
        )

    def piece(step, c, way, first, landed=False):
        start, slots = sets[c]
        source = start.at[way] if first else slots.at[way, step if landed else step - 1]
        return pltpu.make_async_remote_copy(
            src_ref=source,
            dst_ref=slots.at[way, step],
            send_sem=send_sem.at[step, c, way],
            recv_sem=recv_sem.at[step, c, way],
            device_id=((left if way else right), me_tp),
            device_id_type=MESH,
        )

    def gain_piece(away):
        return pltpu.make_async_remote_copy(
            src_ref=gain_slots.at[me_fs],
            dst_ref=gain_slots.at[me_fs],
            send_sem=gain_send.at[away - 1],
            recv_sem=gain_recv.at[away - 1],
            device_id=(lax.rem(me_fs + away, n), me_tp),
            device_id_type=MESH,
        )

    results = ((dnorm_ref, dnorm_out), (mix_ref, mix_out))

    def share(a, away):
        source, target = results[a]
        return pltpu.make_async_remote_copy(
            src_ref=source.at[away - 1],
            dst_ref=target.at[away - 1],
            send_sem=tp_send.at[a, away - 1],
            recv_sem=tp_recv.at[a, away - 1],
            device_id=(me_fs, lax.rem(me_tp + away, n_tp)),
            device_id_type=MESH,
        )

    def keep(a):
        source, target = results[a]
        return pltpu.make_async_copy(source.at[n_tp - 1], target.at[n_tp - 1], own_sem.at[a])

    def block_of(away):
        return pl.ds(pl.multiple_of(lax.rem(me_tp + away, n_tp) * tokens, tokens), tokens)

    def grad_block(away):
        some = block_of(away)
        part = lax.dot_general(
            both_ref[some, :],
            gu_all[...],
            (((1,), (1,)), ((), ())),
            preferred_element_type=jnp.float32,
        ).astype(jnp.bfloat16)
        dnorm_ref[away - 1] = part
        gain_sum[...] += jnp.sum(
            part.astype(jnp.float32) * early_all[some, :].astype(jnp.float32),
            axis=0,
            keepdims=True,
        )

    def late_block(away):
        both = jnp.dot(
            late_all[block_of(away), :], gu_all[...], preferred_element_type=jnp.float32
        )
        gate = both[:, :width]
        hidden = (gate / (1.0 + jnp.exp(-gate)) * both[:, width:]).astype(jnp.bfloat16)
        mix_ref[away - 1] = lax.dot_general(
            hidden, dn_all[...], (((1,), (1,)), ((), ())), preferred_element_type=jnp.float32
        ).astype(jnp.bfloat16)

    for c in range(2):
        for way in range(2):
            sets[c][0][way] = product(0, c, way).astype(jnp.bfloat16)
            piece(0, c, way, True).start()
    gain_sum[...] = jnp.zeros_like(gain_sum)
    for copy in loads:
        copy.wait()

    for c in range(2):
        (grad_block, late_block)[c](1)
        share(c, 1).start()

    def body(step, carry):
        for c in range(2):
            slots = sets[c][1]
            for way in range(2):
                term = product(step, c, way)
                piece(step - 1, c, way, False, True).wait_recv()
                slots[way, step - 1] = (
                    slots[way, step - 1].astype(jnp.float32) + term
                ).astype(jnp.bfloat16)
                piece(step, c, way, False).start()

            @pl.when(step < n_tp)
            def _():
                (grad_block, late_block)[c](step + 1)

            @pl.when(step < n_tp - 1)
            def _():
                share(c, step + 1).start()

            @pl.when(step == n_tp - 1)
            def _():
                keep(c).start()

        @pl.when(step == n_tp - 1)
        def _():
            gain_slots[me_fs] = gain_sum[...] / gain_ref[...]

            def send(away, inner):
                gain_piece(away).start()
                return inner

            lax.fori_loop(1, n, send, 0)

        return carry

    lax.fori_loop(1, n - 1, body, 0)

    def settle(away, inner):
        gain_piece(away).wait()
        return inner

    lax.fori_loop(1, n, settle, 0)
    gain_tp[me_tp] = lax.fori_loop(
        1, n, lambda k, total: total + gain_slots[k], gain_slots[0]
    )
    last = []
    for away in range(1, n_tp):
        peer = lax.rem(me_tp + away, n_tp)
        copy = pltpu.make_async_remote_copy(
            src_ref=gain_tp.at[me_tp],
            dst_ref=gain_tp.at[me_tp],
            send_sem=last_send.at[away - 1],
            recv_sem=last_recv.at[away - 1],
            device_id=(me_fs, peer),
            device_id_type=MESH,
        )
        copy.start()
        last.append(copy)
    for c in range(2):
        slots = sets[c][1]
        for way in range(2):
            term = product(n - 1, c, way)
            piece(n - 2, c, way, False, True).wait_recv()
            total = slots[way, n - 2].astype(jnp.float32) + term
            out = (gu_out, dn_out)[c]
            if turned:
                out[:, pl.ds(way * half, half)] = total.T
            else:
                out[pl.ds(way * half, half), :] = total
            piece(0, c, way, True).wait_send()
    for copy in last:
        copy.wait()
    total = gain_tp[0]
    for k in range(1, n_tp):
        total = total + gain_tp[k]
    gain_out[...] = total

    def drain(step, carry):
        for c in range(2):
            for way in range(2):
                piece(step, c, way, False).wait_send()
        return carry

    lax.fori_loop(1, n - 1, drain, 0)
    for a in range(2):
        keep(a).wait()
        for away in range(1, n_tp):
            share(a, away).wait()


def reduce(n, n_tp, turned, early_side, cot_side, both, hid, gain, early_all, gu_all, dn_all, late_all):
    rows = gu_all.shape[0] // n
    half = rows // 2
    width = dn_all.shape[1]
    shapes = [(rows, 2 * width), (rows, width)]
    if turned:
        shapes = [shape[::-1] for shape in shapes]
    depth = late_all.shape[1]
    tokens = late_all.shape[0] // n_tp
    vmem = pl.BlockSpec(memory_space=pltpu.VMEM)
    hbm = pl.BlockSpec(memory_space=pl.ANY)
    f32, bf16 = jnp.float32, jnp.bfloat16
    return pl.pallas_call(
        functools.partial(reduce_kernel, n, n_tp, turned),
        out_shape=[
            jax.ShapeDtypeStruct(shapes[0], f32),
            jax.ShapeDtypeStruct(shapes[1], f32),
            jax.ShapeDtypeStruct((n_tp, tokens, depth), bf16),
            jax.ShapeDtypeStruct((n_tp, tokens, depth), bf16),
            jax.ShapeDtypeStruct(gain.shape, f32),
        ],
        in_specs=[vmem] * 6 + [hbm] * 3,
        out_specs=[vmem, vmem, hbm, hbm, vmem],
        scratch_shapes=[
            pltpu.VMEM((2, n - 1, half, 2 * width), bf16),
            pltpu.VMEM((2, n - 1, half, width), bf16),
            pltpu.VMEM((n,) + gain.shape, f32),
            pltpu.VMEM((n_tp,) + gain.shape, f32),
            pltpu.VMEM((2, half, 2 * width), bf16),
            pltpu.VMEM((2, half, width), bf16),
            pltpu.VMEM(gu_all.shape, bf16),
            pltpu.VMEM(dn_all.shape, bf16),
            pltpu.VMEM(late_all.shape, bf16),
            pltpu.VMEM((n_tp, tokens, depth), bf16),
            pltpu.VMEM((n_tp, tokens, depth), bf16),
            pltpu.VMEM(gain.shape, f32),
            pltpu.SemaphoreType.DMA((n - 1, 2, 2)),
            pltpu.SemaphoreType.DMA((n - 1, 2, 2)),
            pltpu.SemaphoreType.DMA((n - 1,)),
            pltpu.SemaphoreType.DMA((n - 1,)),
            pltpu.SemaphoreType.DMA((2, n_tp - 1)),
            pltpu.SemaphoreType.DMA((2, n_tp - 1)),
            pltpu.SemaphoreType.DMA((n_tp - 1,)),
            pltpu.SemaphoreType.DMA((n_tp - 1,)),
            pltpu.SemaphoreType.DMA((3,)),
            pltpu.SemaphoreType.DMA((2,)),
        ],
        compiler_params=pltpu.CompilerParams(
            collective_id=1, has_side_effects=True, vmem_limit_bytes=VMEM_LIMIT
        ),
    )(early_side, cot_side, both, hid, gain, early_all, gu_all, dn_all, late_all)


def per_device(
    n,
    n_tp,
    late_input,
    norm_gain,
    gate_weight,
    up_weight,
    down_weight,
    early_input,
    cotangent,
    gate_sum,
    up_sum,
    down_sum,
    gain_sum,
):
    gain_f = norm_gain.astype(jnp.float32)
    width = gate_weight.shape[1]
    depth = late_input.shape[1]
    turned = gate_weight.shape[0] % 256 == 0
    weights = [gate_weight, up_weight, down_weight]
    if turned:
        weights = [weight.T for weight in weights]
    gain_row = gain_f.reshape(1, depth)
    gu_all, down_all, late_all, early_all, cot_all, d_both, hidden_e = gather(
        n, n_tp, turned, *weights, late_input, early_input, cotangent, gain_row
    )
    sides = (early_all, cot_all) if turned else (early_all.T, cot_all.T)
    gu_grad, down_grad, mix_got, d_got, gain_total = reduce(
        n, n_tp, turned, *sides, d_both, hidden_e, gain_row, early_all, gu_all, down_all, late_all
    )
    if turned:
        gate_grad, up_grad, down_grad = gu_grad[:width].T, gu_grad[width:].T, down_grad.T
    else:
        gate_grad, up_grad = gu_grad[:, :width], gu_grad[:, width:]

    def gathered(got):
        total = got[0].astype(jnp.float32)
        for k in range(1, n_tp):
            total = total + got[k].astype(jnp.float32)
        return total

    values = late_input.astype(jnp.float32)
    values_e = early_input.astype(jnp.float32)
    scale_e = lax.rsqrt(jnp.mean(values_e * values_e, axis=-1, keepdims=True) + epsilon)
    late_out = (values + 0.5 * gathered(mix_got)).astype(jnp.bfloat16)
    scaled_grad = gathered(d_got) * gain_f
    early_grad = (
        cotangent.astype(jnp.float32)
        + scale_e * scaled_grad
        - values_e * scale_e**3 * jnp.mean(values_e * scaled_grad, axis=-1, keepdims=True)
    ).astype(jnp.bfloat16)
    return (
        late_out,
        early_grad,
        gate_sum + gate_grad,
        up_sum + up_grad,
        down_sum + down_grad,
        gain_sum + gain_total.reshape(depth),
    )


def solution(mesh):
    token = P(("fs", "tp"), None)
    weight = P("fs", "tp")
    return jax.shard_map(
        functools.partial(per_device, mesh.shape["fs"], mesh.shape["tp"]),
        mesh=mesh,
        in_specs=(token, P(), weight, weight, weight, token, token, weight, weight, weight, P()),
        out_specs=(token, token, weight, weight, weight, P()),
        check_vma=False,
    )
```

profile of v0, /device:TPU:1, one launch (start us, length us, event | category | flops | bytes accessed | tf_op | source)
XLA Modules:
  0.0 198.7 jit_solution(638439002386993822)
XLA Ops:
  0.6 1.3 convert_element_type.51
  1.9 93.6 %shard_map.154 = (bf16[2048,1408]{1,0:T(8,128)(2,1)}, bf16[2048,704]{1,0:T(8,128)(2,1)}, bf16[512,2048]{1,0:T(8,128)(2,1)}, bf16[512,2048]{1,0:T(8,128)(2,1)}, b...) custom-call(bf16[704,256]{1,0:T(8,128)(2,1)} %bitcast.21, ...), custom_call_target="tpu_custom_call" | custom-call | tf_op jit(solution)/shard_map/pallas_call | solution.py:272
  95.6 0.0 copy-start.1
  95.6 0.0 copy-start.2
  95.6 0.0 copy-start.9
  95.6 95.5 %shard_map.155 = (f32[1408,256]{1,0:T(8,128)}, f32[704,256]{1,0:T(8,128)}, bf16[4,128,2048]{2,1,0:T(8,128)(2,1)}, bf16[4,128,2048]{2,1,0:T(8,128)(2,1)}, f32[1,2048]{1,0:T(1,128)}) custom-call(bf16[512,2048]{1,0:T(8,128)(2,1)} %get-tuple-element.18.refs_0_.refs_5_, bf16[512,2048]{1,0:T(8,128)(2,1)} %get-tuple-element.19.refs_1_, ...), custom_call_target="tpu_custom_call" | custom-call | tf_op jit(solution)/shard_map/pallas_call | solution.py:553
  191.2 0.0 copy-done.1
  191.2 0.0 copy-done.2
  191.2 0.0 copy-done.9
  191.2 0.0 copy-start
  191.2 0.0 copy-start.3
  191.2 0.0 copy-start.8
  191.2 3.9 %fusion = (f32[128]{0:T(128)S(1)}, f32[128]{0:T(128)S(1)}, bf16[128,2048]{1,0:T(8,128)(2,1)}) fusion(bf16[128,2048]{1,0:T(8,128)(2,1)S(1)} %copy-done.1, f32[2048]{0:T(1024)S(1)} %copy-done.9, bf16[4,128,2048]{2,1,0:T(8,128)(2,1)} %get-tuple-element.26, bf16[4,128,2048]{2,1,0:T(8,128)(2,1)} %get-tuple-element.25, bf16[128,2048]{1,0:T(8,128)(2,1)S(1)} %copy-done.2), kind=kLoop, calls=%fused_computation.3 | loop fusion | flops 6291200 | bytes 5776384 | tf_op jit(solution)/shard_map/reduce_sum | solution.py:637
  195.1 0.0 copy-start.10
  195.1 0.0 copy-start.11
  195.1 0.0 copy-start.4
  195.1 0.0 copy-start.5
  195.1 0.0 copy-start.6
  195.2 0.0 copy-start.7
  195.2 0.0 copy-done
  195.2 0.0 copy-done.3
  195.2 1.4 fusion.3
  196.6 0.0 copy-done.10
  196.6 0.0 copy-done.11
  196.6 0.6 add.75
  197.2 0.0 copy-done.8
  197.2 0.0 copy-done.4
  197.2 0.0 copy-done.5
  197.2 0.0 copy-done.6
  197.2 0.1 copy-done.7
  197.3 1.4 bitcast_add_fusion.2
  (2 shorter events, 0.0 us)
Async XLA Ops:
  95.6 95.6 %copy-start.1 = (bf16[128,2048]{1,0:T(8,128)(2,1)S(1)}, bf16[128,2048]{1,0:T(8,128)(2,1)}, u32[]{:S(2)}) copy-start(bf16[128,2048]{1,0:T(8,128)(2,1)} %refs_4_.1) | copy-start | bytes 1572868
  95.6 95.6 %copy-start.2 = (bf16[128,2048]{1,0:T(8,128)(2,1)S(1)}, bf16[128,2048]{1,0:T(8,128)(2,1)}, u32[]{:S(2)}) copy-start(bf16[128,2048]{1,0:T(8,128)(2,1)} %refs_3_.1) | copy-start | bytes 1572868
  95.6 95.6 %copy-start.9 = (f32[2048]{0:T(1024)S(1)}, f32[2048]{0:T(1024)}, u32[]{:S(2)}) copy-start(f32[2048]{0:T(1024)} %convert_element_type.51) | copy-start | bytes 24580
  191.2 4.0 %copy-start = (bf16[4,128,2048]{2,1,0:T(8,128)(2,1)S(1)}, bf16[4,128,2048]{2,1,0:T(8,128)(2,1)}, u32[]{:S(2)}) copy-start(bf16[4,128,2048]{2,1,0:T(8,128)(2,1)} %get-tuple-element.26) | copy-start | bytes 6291460
  191.2 4.0 %copy-start.3 = (bf16[128,2048]{1,0:T(8,128)(2,1)S(1)}, bf16[128,2048]{1,0:T(8,128)(2,1)}, u32[]{:S(2)}) copy-start(bf16[128,2048]{1,0:T(8,128)(2,1)} %refs_5_.1) | copy-start | bytes 1572868
  191.2 6.0 %copy-start.8 = (f32[704,256]{1,0:T(8,128)S(1)}, f32[704,256]{1,0:T(8,128)}, u32[]{:S(2)}) copy-start(f32[704,256]{1,0:T(8,128)} %get-tuple-element.28) | copy-start | bytes 2162692
  195.1 1.5 copy-start.10
  195.1 1.5 copy-start.11
  195.1 2.1 %copy-start.4 = (f32[1408,256]{1,0:T(8,128)S(1)}, f32[1408,256]{1,0:T(8,128)}, u32[]{:S(2)}) copy-start(f32[1408,256]{1,0:T(8,128)} %get-tuple-element.27) | copy-start | bytes 4325380
  195.1 2.1 %copy-start.5 = (f32[256,704]{0,1:T(8,128)S(1)}, f32[256,704]{0,1:T(8,128)}, u32[]{:S(2)}) copy-start(f32[256,704]{0,1:T(8,128)} %param.19) | copy-start | bytes 2162692
  195.1 2.1 %copy-start.6 = (f32[256,704]{0,1:T(8,128)S(1)}, f32[256,704]{0,1:T(8,128)}, u32[]{:S(2)}) copy-start(f32[256,704]{0,1:T(8,128)} %param.18) | copy-start | bytes 2162692
  195.2 2.2 %copy-start.7 = (f32[256,704]{0,1:T(8,128)S(1)}, f32[256,704]{0,1:T(8,128)}, u32[]{:S(2)}) copy-start(f32[256,704]{0,1:T(8,128)} %param.20) | copy-start | bytes 2162692
where the time goes:
time: 201 us; the launch traced here: 199 us
  Pallas kernels  189 us (94%)
  other arithmetic  8.6 us (4%)
    pallas_call x1, Pallas kernels, reduce(): pl.pallas_call(functools.partial(reduce_kernel, n, n_tp, turned), out_sha...  95.5 us
    pallas_call x1, Pallas kernels, gather(): pl.pallas_call(functools.partial(gather_kernel, n, n_tp, turned), out_sha...  93.6 us

commit v1 on v0

--- a/solution.py
+++ b/solution.py
@@ -10,6 +10,7 @@
 epsilon = 1e-05
 MESH = pl.DeviceIdType.MESH
 VMEM_LIMIT = 60 * 1024 * 1024
+FUSED_LIMIT = 63 * 1024 * 1024
 
 
 def ring_place(index, n):
@@ -591,7 +592,7 @@
     )(early_side, cot_side, both, hid, gain, early_all, gu_all, dn_all, late_all)
 
 
-def per_device(
+def per_device_rings(
     n,
     n_tp,
     late_input,
@@ -652,6 +653,755 @@
     )
 
 
+def fused_kernel(n, cuts, *refs):
+    gate_in, up_in, dn_in, late_in, early_in, cot_in, gain_ref = refs[:7]
+    sums_in, gain_sum_ref = refs[7:10], refs[10]
+    late_out, early_out = refs[11:13]
+    sum_outs, gain_out = refs[13:16], refs[16]
+    wall, toks, early_raw, late_raw, sums, grad, pair, slots = refs[17:25]
+    act_f, act_t, d_gate, d_up, hid_l, part = refs[25:31]
+    from_x, from_y, diag_x, diag_y, gain_mine, gain_got, gain_z = refs[31:38]
+    back_mine, back_got, back_send, back_recv = refs[38:42]
+    load_sem, own_sem, swap_send, swap_recv, line_send, line_recv = refs[42:48]
+    core_send, core_recv, tok_send, tok_recv, pair_send, pair_recv = refs[48:54]
+    rs_send, rs_recv, xy_send, xy_recv, gain_send, gain_recv = refs[54:]
+    nz = n // 2
+    fs, tp = lax.axis_index("fs"), lax.axis_index("tp")
+    z, x = fs // 2, lax.rem(fs, 2)
+    y, c = tp // 2, lax.rem(tp, 2)
+    weights = (gate_in, up_in, dn_in)
+    tokens, depth = late_in.shape
+    width, rows = gate_in.shape
+    split = tokens // 2
+    bf16, f32 = jnp.bfloat16, jnp.float32
+    count = len(cuts)
+    straight = x == c
+
+    def at(z_at, x_at, y_at, c_at):
+        return (2 * z_at + x_at, 2 * y_at + c_at)
+
+    up_z, down_z = lax.rem(z + 1, nz), lax.rem(z + nz - 1, nz)
+    partner = at(z, x, y, 1 - c)
+    x_side = at(z, 1 - x, y, c)
+    y_side = at(z, x, 1 - y, c)
+    crossed = at(z, c, y, x)
+
+    def send(source, target, send_sem, recv_sem, device):
+        return pltpu.make_async_remote_copy(
+            src_ref=source,
+            dst_ref=target,
+            send_sem=send_sem,
+            recv_sem=recv_sem,
+            device_id=device,
+            device_id_type=MESH,
+        )
+
+    def hold(k):
+        return pl.ds(cuts[k][0], cuts[k][1])
+
+    def block(j, wide=1):
+        return pl.ds(pl.multiple_of(j * rows, rows), wide * rows)
+
+    def some(start, size):
+        return pl.ds(pl.multiple_of(start, 16), size)
+
+    def own_load(k, m):
+        return pltpu.make_async_copy(
+            weights[m].at[hold(k)], wall.at[m, hold(k), block(fs)], own_sem.at[k, m]
+        )
+
+    def swap(k, m):
+        return send(
+            weights[m].at[hold(k)],
+            wall.at[m, hold(k), block(fs)],
+            swap_send.at[k, m],
+            swap_recv.at[k, m],
+            crossed,
+        )
+
+    p_me, p_x, p_y = 2 * x + y, 2 * (1 - x) + y, 2 * x + 1 - y
+    p_d = 3 - p_me
+
+    def place(p, start=0, size=tokens):
+        return some(p * tokens + start, size)
+
+    loads = [
+        pltpu.make_async_copy(source, target, load_sem.at[i])
+        for i, (source, target) in enumerate(
+            (
+                (early_in, early_raw),
+                (late_in, late_raw),
+                (cot_in, toks.at[1, place(p_me)]),
+                (sums_in[0], sums.at[0]),
+                (sums_in[1], sums.at[1]),
+                (sums_in[2], sums.at[2]),
+            )
+        )
+    ]
+    for copy in loads[:3]:
+        copy.start()
+
+    @pl.when(straight)
+    def _():
+        for k in range(count):
+            for m in range(3):
+                own_load(k, m).start()
+
+    for copy in loads[3:]:
+        copy.start()
+
+    barrier = pltpu.get_barrier_semaphore()
+
+    def greet_at(device):
+        pl.semaphore_signal(barrier, inc=1, device_id=device, device_id_type=MESH)
+
+    for away in range(1, nz):
+        greet_at(at(lax.rem(z + away, nz), x, y, c))
+    for device in (partner, x_side, y_side):
+        greet_at(device)
+
+    @pl.when(straight)
+    def _():
+        pl.semaphore_wait(barrier, nz - 1 + 3)
+
+    @pl.when(x != c)
+    def _():
+        greet_at(crossed)
+        pl.semaphore_wait(barrier, nz - 1 + 4)
+
+    def tok(a, kind):
+        if kind < 2:
+            where = place(p_me)
+        elif kind == 2:
+            where = place(p_y, 0, split)
+        else:
+            where = place(p_x, split, tokens - split)
+        spot = toks.at[a, where]
+        source = cot_in if a == 1 and kind < 2 else spot
+        return send(
+            source, spot, tok_send.at[a, kind], tok_recv.at[a, kind], y_side if kind % 2 else x_side
+        )
+
+    def tok_forward(a):
+        tok(a, 1).wait_recv()
+        tok(a, 2).start()
+        tok(a, 0).wait_recv()
+        tok(a, 3).start()
+
+    def tok_rest(a):
+        tok(a, 2).wait_recv()
+        tok(a, 3).wait_recv()
+
+    def line(k, zs, way, dist):
+        spot = wall.at[:, hold(k), block(2 * zs + c)]
+        return send(
+            spot,
+            spot,
+            line_send.at[k, way, dist - 1],
+            line_recv.at[k, way, dist - 1],
+            at(down_z if way else up_z, x, y, c),
+        )
+
+    def core_copy(k, zs):
+        spot = wall.at[:, hold(k), block(2 * zs + c)]
+        return send(spot, spot, core_send.at[k, zs], core_recv.at[k, zs], partner)
+
+    def pump(k, d):
+        if d == 0:
+
+            @pl.when(straight)
+            def _():
+                for m in range(3):
+                    own_load(k, m).wait()
+
+            @pl.when(x != c)
+            def _():
+                for m in range(3):
+                    swap(k, m).wait_recv()
+
+            @pl.when(z < nz - 1)
+            def _():
+                line(k, z, 0, 1).start()
+
+            @pl.when(z > 0)
+            def _():
+                line(k, z, 1, 1).start()
+
+            core_copy(k, z).start()
+            return
+
+        @pl.when(z >= d)
+        def _():
+            line(k, z - d, 0, d).wait_recv()
+
+            if d < nz - 1:
+
+                @pl.when(z < nz - 1)
+                def _():
+                    line(k, z - d, 0, d + 1).start()
+
+            core_copy(k, z - d).start()
+
+        @pl.when(z + d < nz)
+        def _():
+            line(k, z + d, 1, d).wait_recv()
+
+            if d < nz - 1:
+
+                @pl.when(z > 0)
+                def _():
+                    line(k, z + d, 1, d + 1).start()
+
+            core_copy(k, z + d).start()
+
+    def weights_in(k):
+        for zs in range(nz):
+            core_copy(k, zs).wait_recv()
+
+    def norm(source, a):
+        def step(i, carry):
+            values = source[some(i * 16, 16), :].astype(f32)
+            scale = lax.rsqrt(jnp.mean(values * values, axis=-1, keepdims=True) + epsilon)
+            toks[a, some(p_me * tokens + i * 16, 16), :] = (
+                values * scale * gain_ref[...]
+            ).astype(bf16)
+            return carry
+
+        lax.fori_loop(0, tokens // 16, step, 0)
+
+    def dot(left, right, sides):
+        return lax.dot_general(left, right, (sides, ((), ())), preferred_element_type=f32)
+
+    def hidden_dots(k, pairs):
+        size = cuts[k][1]
+        for i, (a, m) in enumerate(pairs):
+            act_f[i, :, :size] = dot(toks[a], wall[m, hold(k), :], ((1,), (1,)))
+
+    def act_early(k):
+        size = cuts[k][1]
+        hidden_dots(k, ((0, 0), (0, 1), (1, 2)))
+
+        def step(i, carry):
+            part_of = pl.ds(pl.multiple_of(i * 128, 128), 128)
+            gate, upper = act_f[0, part_of, :size], act_f[1, part_of, :size]
+            sigma = 1.0 / (1.0 + jnp.exp(-gate))
+            d_hidden = 0.5 * act_f[2, part_of, :size]
+            hidden = (gate * sigma * upper).astype(bf16)
+            dg = (d_hidden * upper * sigma * (1.0 + gate * (1.0 - sigma))).astype(bf16)
+            du = (d_hidden * gate * sigma).astype(bf16)
+            d_gate[part_of, hold(k)] = dg
+            d_up[part_of, hold(k)] = du
+            act_t[0, hold(k), part_of] = dg.T
+            act_t[1, hold(k), part_of] = du.T
+            act_t[2, hold(k), part_of] = hidden.T
+            return carry
+
+        lax.fori_loop(0, 4 * tokens // 128, step, 0)
+
+    def act_late(k):
+        size = cuts[k][1]
+        hidden_dots(k, ((2, 0), (2, 1)))
+
+        def step(i, carry):
+            part_of = pl.ds(pl.multiple_of(i * 64, 64), 64)
+            gate, upper = act_f[0, part_of, :size], act_f[1, part_of, :size]
+            hid_l[part_of, hold(k)] = (gate / (1.0 + jnp.exp(-gate)) * upper).astype(bf16)
+            return carry
+
+        lax.fori_loop(0, 4 * tokens // 64, step, 0)
+
+    def turn(i):
+        near = (1 - lax.rem(i, 2)) * (nz - 1 - i // 2) + lax.rem(i, 2) * (i // 2)
+        far = (z >= nz // 2).astype(jnp.int32)
+        return (1 - far) * near + far * (nz - 1 - near)
+
+    def pair_copy(k, zq):
+        return send(
+            grad.at[:, hold(k), block(2 * zq + 1 - c)],
+            pair.at[:, hold(k), block(zq)],
+            pair_send.at[k, zq],
+            pair_recv.at[k, zq],
+            partner,
+        )
+
+    def products(k):
+        def step(i, carry):
+            zq = turn(i)
+            both = block(2 * zq, 2)
+            for m in range(3):
+                grad[m, hold(k), both] = dot(
+                    act_t[m, hold(k), :], toks[m // 2, :, both], ((1,), (0,))
+                ).astype(bf16)
+            pair_copy(k, zq).start()
+            return carry
+
+        lax.fori_loop(0, nz, step, 0)
+
+    def passing(k, zq, way):
+        if way == 0:
+            target, slot = up_z, zq
+        else:
+            last = (zq == z - 1).astype(jnp.int32)
+            target, slot = down_z, last * nz + (1 - last) * zq
+        return send(
+            grad.at[:, hold(k), block(2 * zq + c)],
+            slots.at[slot, :, hold(k), :],
+            rs_send.at[k, zq],
+            rs_recv.at[k, slot],
+            at(target, x, y, c),
+        )
+
+    def landed(k, slot):
+        here = slots.at[slot, :, hold(k), :]
+        return send(here, here, rs_send.at[k, 0], rs_recv.at[k, slot], partner)
+
+    def pass_on(k, zq):
+        @pl.when(zq > z)
+        def _():
+            passing(k, zq, 0).start()
+
+        @pl.when(zq < z)
+        def _():
+            passing(k, zq, 1).start()
+
+    def upstream(zq):
+        return ((zq > z) & (z > 0)) | ((zq < z) & (z < nz - 1))
+
+    def combine_free(k):
+        def step(i, carry):
+            zq = turn(i)
+
+            @pl.when((zq != z) & jnp.logical_not(upstream(zq)))
+            def _():
+                pair_copy(k, zq).wait_recv()
+                for m in range(3):
+                    spot = (m, hold(k), block(2 * zq + c))
+                    grad[spot] = (
+                        grad[spot].astype(f32) + pair[m, hold(k), block(zq)].astype(f32)
+                    ).astype(bf16)
+                pass_on(k, zq)
+
+            return carry
+
+        lax.fori_loop(0, nz, step, 0)
+
+    def combine_up(k, i):
+        zq = turn(jnp.int32(i))
+
+        @pl.when((zq != z) & upstream(zq))
+        def _():
+            pair_copy(k, zq).wait_recv()
+            landed(k, zq).wait_recv()
+            for m in range(3):
+                spot = (m, hold(k), block(2 * zq + c))
+                grad[spot] = (
+                    grad[spot].astype(f32)
+                    + pair[m, hold(k), block(zq)].astype(f32)
+                    + slots[zq, m, hold(k), :].astype(f32)
+                ).astype(bf16)
+            pass_on(k, zq)
+
+    def back(k):
+        spot = back_mine.at[:, hold(k), :]
+        return send(
+            spot, back_got.at[:, hold(k), :], back_send.at[k], back_recv.at[k], crossed
+        )
+
+    factors = (1.0, 1.0, 0.5)
+
+    def finish(k):
+        pair_copy(k, z).wait_recv()
+
+        @pl.when(z > 0)
+        def _():
+            landed(k, z).wait_recv()
+
+        @pl.when(z < nz - 1)
+        def _():
+            landed(k, nz).wait_recv()
+
+        def total(m):
+            return (
+                grad[m, hold(k), block(2 * z + c)].astype(f32)
+                + pair[m, hold(k), block(z)].astype(f32)
+                + slots[z, m, hold(k), :].astype(f32)
+                + slots[nz, m, hold(k), :].astype(f32)
+            )
+
+        @pl.when(straight)
+        def _():
+            for m in range(3):
+                sum_outs[m][hold(k), :] = sums[m, hold(k), :] + factors[m] * total(m)
+
+        @pl.when(x != c)
+        def _():
+            for m in range(3):
+                back_mine[m, hold(k), :] = total(m).astype(bf16)
+            back(k).start()
+
+    def finish_back(k):
+        @pl.when(x != c)
+        def _():
+            back(k).wait_recv()
+            for m in range(3):
+                sum_outs[m][hold(k), :] = sums[m, hold(k), :] + factors[m] * back_got[
+                    m, hold(k), :
+                ].astype(f32)
+
+    low, high = (0, split), (split, tokens - split)
+
+    def share(a, kind):
+        def of(p, piece):
+            return part.at[a, place(p, *piece)]
+
+        source, target = (
+            (of(p_d, low), diag_x.at[a]),
+            (of(p_d, high), diag_y.at[a]),
+            (of(p_x, low), from_x.at[a, pl.ds(*low)]),
+            (of(p_y, high), from_y.at[a, pl.ds(*high)]),
+            (of(p_x, high), from_x.at[a, pl.ds(*high)]),
+            (of(p_y, low), from_y.at[a, pl.ds(*low)]),
+        )[kind]
+        device = (x_side, y_side, x_side, y_side, x_side, y_side)[kind]
+        return send(source, target, xy_send.at[a, kind], xy_recv.at[a, kind], device)
+
+    def half_of(side):
+        return pl.ds(pl.multiple_of(side * 2 * tokens, 2 * tokens), 2 * tokens)
+
+    def grad_half(side):
+        where = half_of(side)
+        both = (
+            dot(d_gate[where, :], wall[0], ((1,), (0,)))
+            + dot(d_up[where, :], wall[1], ((1,), (0,)))
+        ).astype(bf16)
+        part[0, where, :] = both
+
+    def gain_half(side):
+        def step(i, total):
+            where = some(side * 2 * tokens + i * 16, 16)
+            term = part[0, where, :].astype(f32) * toks[0, where, :].astype(f32)
+            return total + term[:8] + term[8:]
+
+        return lax.fori_loop(0, tokens // 8, step, jnp.zeros((8, depth), f32))
+
+    def late_half(side):
+        where = half_of(side)
+        part[1, where, :] = dot(hid_l[where, :], wall[2], ((1,), (0,))).astype(bf16)
+
+    def share_forward(a):
+        share(a, 1).wait_recv()
+        where = place(p_x, *high)
+        part[a, where, :] = (part[a, where, :].astype(f32) + diag_y[a].astype(f32)).astype(bf16)
+        share(a, 4).start()
+        share(a, 0).wait_recv()
+        where = place(p_y, *low)
+        part[a, where, :] = (part[a, where, :].astype(f32) + diag_x[a].astype(f32)).astype(bf16)
+        share(a, 5).start()
+
+    def share_in(a):
+        for kind in range(2, 6):
+            share(a, kind).wait_recv()
+
+    def own_total(a, i):
+        where, mine = some(i * 16, 16), some(p_me * tokens + i * 16, 16)
+        return (
+            part[a, mine, :].astype(f32)
+            + from_x[a, where, :].astype(f32)
+            + from_y[a, where, :].astype(f32)
+        )
+
+    def write_late():
+        def step(i, carry):
+            where = some(i * 16, 16)
+            late_out[where, :] = (
+                late_raw[where, :].astype(f32) + 0.5 * own_total(1, i)
+            ).astype(bf16)
+            return carry
+
+        lax.fori_loop(0, tokens // 16, step, 0)
+
+    def write_early():
+        def step(i, carry):
+            where = some(i * 16, 16)
+            values = early_raw[where, :].astype(f32)
+            scale = lax.rsqrt(jnp.mean(values * values, axis=-1, keepdims=True) + epsilon)
+            scaled = own_total(0, i) * gain_ref[...]
+            mean = jnp.mean(values * scaled, axis=-1, keepdims=True)
+            cot = toks[1, some(p_me * tokens + i * 16, 16), :].astype(f32)
+            early_out[where, :] = (cot + scale * scaled - values * scale**3 * mean).astype(bf16)
+            return carry
+
+        lax.fori_loop(0, tokens // 16, step, 0)
+
+    def gain_step(i):
+        return send(
+            gain_mine.at[i],
+            gain_got.at[i],
+            gain_send.at[i],
+            gain_recv.at[i],
+            (partner, x_side, y_side)[i],
+        )
+
+    def gain_away(away):
+        return send(
+            gain_z.at[z],
+            gain_z.at[z],
+            gain_send.at[2 + away],
+            gain_recv.at[2 + away],
+            at(lax.rem(z + away, nz), x, y, c),
+        )
+
+    def gain_next(i):
+        gain_step(i).wait_recv()
+        total = gain_mine[i] + gain_got[i]
+        if i < 2:
+            gain_mine[i + 1] = total
+            gain_step(i + 1).start()
+        else:
+            gain_z[z] = total
+            for away in range(1, nz):
+                gain_away(away).start()
+
+    @pl.when(x != c)
+    def _():
+        for m in range(3):
+            swap(0, m).start()
+
+    tok(1, 0).start()
+    tok(1, 1).start()
+    loads[0].wait()
+    norm(early_raw, 0)
+    tok(0, 0).start()
+    tok(0, 1).start()
+    pump(0, 0)
+    loads[1].wait()
+    norm(late_raw, 2)
+
+    @pl.when(z == 0)
+    def _():
+        slots[0] = jnp.zeros_like(slots[0])
+
+    @pl.when(z == nz - 1)
+    def _():
+        slots[nz] = jnp.zeros_like(slots[nz])
+
+    tok_forward(1)
+    pump(0, 1)
+    tok_forward(0)
+
+    @pl.when(x != c)
+    def _():
+        for k in range(1, count):
+            for m in range(3):
+                swap(k, m).start()
+
+    tok(2, 0).start()
+    tok(2, 1).start()
+    for d in range(2, nz):
+        pump(0, d)
+    if count > 1:
+        pump(1, 0)
+    loads[2].wait()
+    tok_rest(1)
+    tok_rest(0)
+    for k in range(count):
+        weights_in(k)
+        act_early(k)
+        products(k)
+        combine_free(k)
+        if k == 0:
+            tok_forward(2)
+        if k < count - 1:
+            for d in range(1, nz):
+                pump(k + 1, d)
+                combine_up(k, d - 1)
+                if d == 1:
+                    if k == 0:
+                        tok_rest(2)
+                    act_late(k)
+            combine_up(k, nz - 1)
+            if k + 2 < count:
+                pump(k + 2, 0)
+    if count == 1:
+        tok_rest(2)
+    act_late(count - 1)
+    grad_half(1 - x)
+    for kind in range(3):
+        share(0, kind).start()
+    late_half(1 - x)
+    for kind in range(3):
+        share(1, kind).start()
+    grad_half(x)
+    share(0, 3).start()
+    late_half(x)
+    share(1, 3).start()
+    gain = jnp.sum(gain_half(1 - x) + gain_half(x), axis=0, keepdims=True)
+    gain_mine[0] = gain / gain_ref[...]
+    gain_step(0).start()
+    for i in range(3):
+        loads[3 + i].wait()
+    for k in range(count - 1):
+        finish(k)
+    combine_up(count - 1, 0)
+    share_forward(0)
+    gain_next(0)
+    combine_up(count - 1, 1)
+    share_forward(1)
+    gain_next(1)
+    for i in range(2, nz):
+        combine_up(count - 1, i)
+    gain_next(2)
+    share_in(0)
+    write_early()
+    share_in(1)
+    write_late()
+    for away in range(1, nz):
+        gain_away(away).wait_recv()
+    total = gain_z[0]
+    for k in range(1, nz):
+        total = total + gain_z[k]
+    gain_out[...] = gain_sum_ref[...] + total
+    finish(count - 1)
+    for k in range(count):
+        finish_back(k)
+
+    for i in range(3):
+        gain_step(i).wait_send()
+    for away in range(1, nz):
+        gain_away(away).wait_send()
+    for a in range(3):
+        for kind in range(4):
+            tok(a, kind).wait_send()
+    for a in range(2):
+        for kind in range(6):
+            share(a, kind).wait_send()
+    for k in range(count):
+
+        @pl.when(x != c)
+        def _():
+            for m in range(3):
+                swap(k, m).wait_send()
+            back(k).wait_send()
+
+        for d in range(nz - 1):
+
+            @pl.when((z >= d) & (z < nz - 1))
+            def _():
+                line(k, z - d, 0, d + 1).wait_send()
+
+            @pl.when((z + d < nz) & (z > 0))
+            def _():
+                line(k, z + d, 1, d + 1).wait_send()
+
+        for zs in range(nz):
+            core_copy(k, zs).wait_send()
+            pair_copy(k, zs).wait_send()
+
+            @pl.when(zs != z)
+            def _():
+                passing(k, jnp.int32(zs), 0).wait_send()
+
+
+def fused(n, cuts, gate, up, dn, late, early, cot, gain, sums, gain_sum):
+    width, rows = gate.shape
+    tokens, depth = late.shape
+    nz, count = n // 2, len(cuts)
+    most = max(size for _, size in cuts)
+    vmem = pl.BlockSpec(memory_space=pltpu.VMEM)
+    hbm = pl.BlockSpec(memory_space=pl.ANY)
+    f32, bf16 = jnp.float32, jnp.bfloat16
+    dma = pltpu.SemaphoreType.DMA
+    crowd = 4 * tokens
+    split = tokens // 2
+    return pl.pallas_call(
+        functools.partial(fused_kernel, n, cuts),
+        out_shape=[jax.ShapeDtypeStruct((tokens, depth), bf16)] * 2
+        + [jax.ShapeDtypeStruct((width, rows), f32)] * 3
+        + [jax.ShapeDtypeStruct((1, depth), f32)],
+        in_specs=[hbm] * 6 + [vmem] + [hbm] * 3 + [vmem],
+        out_specs=[vmem] * 6,
+        scratch_shapes=[
+            pltpu.VMEM((3, width, depth), bf16),
+            pltpu.VMEM((3, crowd, depth), bf16),
+            pltpu.VMEM((tokens, depth), bf16),
+            pltpu.VMEM((tokens, depth), bf16),
+            pltpu.VMEM((3, width, rows), f32),
+            pltpu.VMEM((3, width, depth), bf16),
+            pltpu.VMEM((3, width, nz * rows), bf16),
+            pltpu.VMEM((nz + 1, 3, width, rows), bf16),
+            pltpu.VMEM((3, crowd, most), f32),
+            pltpu.VMEM((3, width, crowd), bf16),
+            pltpu.VMEM((crowd, width), bf16),
+            pltpu.VMEM((crowd, width), bf16),
+            pltpu.VMEM((crowd, width), bf16),
+            pltpu.VMEM((2, crowd, depth), bf16),
+            pltpu.VMEM((2, tokens, depth), bf16),
+            pltpu.VMEM((2, tokens, depth), bf16),
+            pltpu.VMEM((2, split, depth), bf16),
+            pltpu.VMEM((2, tokens - split, depth), bf16),
+            pltpu.VMEM((3, 1, depth), f32),
+            pltpu.VMEM((3, 1, depth), f32),
+            pltpu.VMEM((nz, 1, depth), f32),
+            pltpu.VMEM((3, width, rows), bf16),
+            pltpu.VMEM((3, width, rows), bf16),
+            dma((count,)),
+            dma((count,)),
+            dma((6,)),
+            dma((count, 3)),
+            dma((count, 3)),
+            dma((count, 3)),
+            dma((count, 2, nz - 1)),
+            dma((count, 2, nz - 1)),
+            dma((count, nz)),
+            dma((count, nz)),
+            dma((3, 4)),
+            dma((3, 4)),
+            dma((count, nz)),
+            dma((count, nz)),
+            dma((count, nz)),
+            dma((count, nz + 1)),
+            dma((2, 6)),
+            dma((2, 6)),
+            dma((2 + nz,)),
+            dma((2 + nz,)),
+        ],
+        compiler_params=pltpu.CompilerParams(
+            collective_id=2, has_side_effects=True, vmem_limit_bytes=FUSED_LIMIT
+        ),
+    )(gate, up, dn, late, early, cot, gain, *sums, gain_sum)
+
+
+def cut_hidden(width):
+    first = min(width, -(-width // 256) * 128)
+    return tuple(cut for cut in ((0, first), (first, width - first)) if cut[1])
+
+
+def per_device_fused(n, args):
+    late, norm_gain, gate, up, dn, early, cot, gate_sum, up_sum, dn_sum, gain_sum = args
+    depth = late.shape[1]
+    out = fused(
+        n,
+        cut_hidden(gate.shape[1]),
+        gate.T,
+        up.T,
+        dn.T,
+        late,
+        early,
+        cot,
+        norm_gain.astype(jnp.float32).reshape(1, depth),
+        (gate_sum.T, up_sum.T, dn_sum.T),
+        gain_sum.reshape(1, depth),
+    )
+    late_out, early_grad, gate_out, up_out, dn_out, gain_out = out
+    return late_out, early_grad, gate_out.T, up_out.T, dn_out.T, gain_out.reshape(depth)
+
+
+def per_device(n, n_tp, *args):
+    if n_tp == 4 and n % 2 == 0 and args[2].shape[0] % 128 == 0:
+        return per_device_fused(n, args)
+    return per_device_rings(n, n_tp, *args)
+
+
 def solution(mesh):
     token = P(("fs", "tp"), None)
     weight = P("fs", "tp")

time: 201 us -> 174 us (0.87)
  Pallas kernels: 189 us -> 164 us
  other arithmetic: 8.6 us -> 0.6 us
  local copies, waits for them, and re-layouts: 0.18 us -> 8.12 us
    pallas_call x2 -> x1, Pallas kernels: 189 us -> 164 us  [fused(): pl.pallas_call(functools.partial(fused_kernel, n, cuts), out_shape=[jax.S...]
    unnamed x24 -> x18, local copies, waits for them, and re-layouts: 0.18 us -> 8.12 us
    reduce_sum x1 -> x0, other arithmetic: 3.91 us -> none  [per_device(): jnp.mean(values_e * values_e, axis=-1, keepdims=True) + epsilon]
    convert_element_type x2 -> x0, other arithmetic: 2.65 us -> none  [the longest x1 1.37 us: per_device(): early_grad = (cotangent.astype(jnp.float32) + scale_e * scaled_grad - val...]
    add x2 -> x0, other arithmetic: 2.03 us -> none  [the longest x1 1.42 us: per_device(): up_sum + up_grad]
where the time goes in v1:
time: 174 us; the launch traced here: 173 us
  Pallas kernels  164 us (94%)
  local copies, waits for them, and re-layouts  8.12 us (5%)
    pallas_call x1, Pallas kernels, fused(): pl.pallas_call(functools.partial(fused_kernel, n, cuts), out_shape=[jax.S...  164 us
    unnamed x18, local copies, waits for them, and re-layouts  8.12 us

profile of v1, /device:TPU:1, one launch (start us, length us, event | category | flops | bytes accessed | tf_op | source)
XLA Modules:
  0.0 173.3 jit_solution(15758147161422786463)
XLA Ops:
  0.6 0.0 copy-start.5
  0.6 0.7 copy-done.5
  1.3 0.6 reshape.27
  1.9 163.9 %shard_map.154 = (bf16[128,2048]{1,0:T(8,128)(2,1)}, bf16[128,2048]{1,0:T(8,128)(2,1)}, f32[704,256]{1,0:T(8,128)}, f32[704,256]{1,0:T(8,128)}, f32[704,256]{1,0:T(8,128)}, /*index=5*/f32[1,2048]{1,0:T(1,128)}) custom-call(bf16[704,256]{1,0:T(8,128)(2,1)} %bitcast.18, bf16[704,256]{1,0:T(8,128)(2,1)} %bitcast.19, bf16[704,256]{1,0:T(8,128)(2,1)} %bitcast.20, ...), custom_call_target="tpu_custom_call" | custom-call | tf_op jit(solution)/shard_map/pallas_call | solution.py:1316
  165.8 0.0 copy-start.3
  165.8 1.9 %copy.23 = bf16[128,2048]{1,0:T(8,128)(2,1)} copy(bf16[128,2048]{1,0:T(8,128)(2,1)} %get-tuple-element.24) | data formatting | bytes 1048576
  167.8 0.0 copy-done.3
  167.8 0.0 copy-start.2
  167.8 0.8 copy.24
  168.6 0.5 copy-done.2
  169.1 0.0 copy-start.1
  169.1 0.9 copy.25
  169.9 0.5 copy-done.1
  170.5 0.0 copy-start
  170.5 0.9 copy.26
  171.3 0.5 copy-done
  171.8 0.0 copy-start.4
  171.8 0.9 copy.27
  172.7 0.0 copy-done.4
  172.7 0.6 copy.28
Async XLA Ops:
  0.6 0.7 copy-start.5
  165.8 2.0 %copy-start.3 = (bf16[128,2048]{1,0:T(8,128)(2,1)S(1)}, bf16[128,2048]{1,0:T(8,128)(2,1)}, u32[]{:S(2)}) copy-start(bf16[128,2048]{1,0:T(8,128)(2,1)} %get-tuple-element.25) | copy-start | bytes 1572868
  167.8 1.3 copy-start.2
  169.1 1.4 copy-start.1
  170.5 1.4 copy-start
  171.8 0.9 copy-start.4

commit v2 on v1

--- a/solution.py
+++ b/solution.py
@@ -656,15 +656,15 @@
 def fused_kernel(n, cuts, *refs):
     gate_in, up_in, dn_in, late_in, early_in, cot_in, gain_ref = refs[:7]
     sums_in, gain_sum_ref = refs[7:10], refs[10]
-    late_out, early_out = refs[11:13]
-    sum_outs, gain_out = refs[13:16], refs[16]
+    token_outs, sum_outs, gain_out = refs[11:13], refs[13:16], refs[16]
     wall, toks, early_raw, late_raw, sums, grad, pair, slots = refs[17:25]
     act_f, act_t, d_gate, d_up, hid_l, part = refs[25:31]
     from_x, from_y, diag_x, diag_y, gain_mine, gain_got, gain_z = refs[31:38]
     back_mine, back_got, back_send, back_recv = refs[38:42]
+    token_sem, sum_sem, gain_sem, gain_f = refs[-4:]
     load_sem, own_sem, swap_send, swap_recv, line_send, line_recv = refs[42:48]
     core_send, core_recv, tok_send, tok_recv, pair_send, pair_recv = refs[48:54]
-    rs_send, rs_recv, xy_send, xy_recv, gain_send, gain_recv = refs[54:]
+    rs_send, rs_recv, xy_send, xy_recv, gain_send, gain_recv = refs[54:-4]
     nz = n // 2
     fs, tp = lax.axis_index("fs"), lax.axis_index("tp")
     z, x = fs // 2, lax.rem(fs, 2)
@@ -672,7 +672,8 @@
     weights = (gate_in, up_in, dn_in)
     tokens, depth = late_in.shape
     width, rows = gate_in.shape
-    split = tokens // 2
+    split = tokens * 3 // 128 * 16
+    tok_splits = (16, split, tokens // 2)
     bf16, f32 = jnp.bfloat16, jnp.float32
     count = len(cuts)
     straight = x == c
@@ -760,31 +761,29 @@
     for device in (partner, x_side, y_side):
         greet_at(device)
 
-    @pl.when(straight)
-    def _():
-        pl.semaphore_wait(barrier, nz - 1 + 3)
-
     @pl.when(x != c)
     def _():
         greet_at(crossed)
-        pl.semaphore_wait(barrier, nz - 1 + 4)
 
     def tok(a, kind):
+        cut = tok_splits[a]
         if kind < 2:
             where = place(p_me)
         elif kind == 2:
-            where = place(p_y, 0, split)
+            where = place(p_y, 0, cut)
         else:
-            where = place(p_x, split, tokens - split)
+            where = place(p_x, cut, tokens - cut)
         spot = toks.at[a, where]
         source = cot_in if a == 1 and kind < 2 else spot
         return send(
             source, spot, tok_send.at[a, kind], tok_recv.at[a, kind], y_side if kind % 2 else x_side
         )
 
-    def tok_forward(a):
+    def tok_over_x(a):
         tok(a, 1).wait_recv()
         tok(a, 2).start()
+
+    def tok_over_y(a):
         tok(a, 0).wait_recv()
         tok(a, 3).start()
 
@@ -819,14 +818,6 @@
                 for m in range(3):
                     swap(k, m).wait_recv()
 
-            @pl.when(z < nz - 1)
-            def _():
-                line(k, z, 0, 1).start()
-
-            @pl.when(z > 0)
-            def _():
-                line(k, z, 1, 1).start()
-
             core_copy(k, z).start()
             return
 
@@ -853,6 +844,23 @@
                     line(k, z + d, 1, d + 1).start()
 
             core_copy(k, z + d).start()
+
+    def lead(k):
+        pump(k, 0)
+
+        @pl.when(z == 0)
+        def _():
+            line(k, z, 0, 1).start()
+
+        @pl.when(z == nz - 1)
+        def _():
+            line(k, z, 1, 1).start()
+
+    def follow(k):
+        @pl.when((z < nz - 1) & (z > 0))
+        def _():
+            line(k, z, 0, 1).start()
+            line(k, z, 1, 1).start()
 
     def weights_in(k):
         for zs in range(nz):
@@ -863,7 +871,7 @@
             values = source[some(i * 16, 16), :].astype(f32)
             scale = lax.rsqrt(jnp.mean(values * values, axis=-1, keepdims=True) + epsilon)
             toks[a, some(p_me * tokens + i * 16, 16), :] = (
-                values * scale * gain_ref[...]
+                values * scale * gain_f[...]
             ).astype(bf16)
             return carry
 
@@ -872,14 +880,17 @@
     def dot(left, right, sides):
         return lax.dot_general(left, right, (sides, ((), ())), preferred_element_type=f32)
 
-    def hidden_dots(k, pairs):
+    def hidden_dots(k, triples):
         size = cuts[k][1]
-        for i, (a, m) in enumerate(pairs):
+        for i, a, m in triples:
             act_f[i, :, :size] = dot(toks[a], wall[m, hold(k), :], ((1,), (1,)))
 
-    def act_early(k):
+    def act_first(k):
+        hidden_dots(k, ((0, 0, 0), (1, 0, 1)))
+
+    def act_second(k):
         size = cuts[k][1]
-        hidden_dots(k, ((0, 0), (0, 1), (1, 2)))
+        hidden_dots(k, ((2, 1, 2),))
 
         def step(i, carry):
             part_of = pl.ds(pl.multiple_of(i * 128, 128), 128)
@@ -900,7 +911,7 @@
 
     def act_late(k):
         size = cuts[k][1]
-        hidden_dots(k, ((2, 0), (2, 1)))
+        hidden_dots(k, ((0, 2, 0), (1, 2, 1)))
 
         def step(i, carry):
             part_of = pl.ds(pl.multiple_of(i * 64, 64), 64)
@@ -928,11 +939,16 @@
         def step(i, carry):
             zq = turn(i)
             both = block(2 * zq, 2)
+            gains = jnp.zeros((1, 2 * rows), f32)
             for m in range(3):
-                grad[m, hold(k), both] = dot(
-                    act_t[m, hold(k), :], toks[m // 2, :, both], ((1,), (0,))
-                ).astype(bf16)
+                term = dot(act_t[m, hold(k), :], toks[m // 2, :, both], ((1,), (0,)))
+                grad[m, hold(k), both] = term.astype(bf16)
+                if m < 2:
+                    gains += jnp.sum(
+                        term * wall[m, hold(k), both].astype(f32), axis=0, keepdims=True
+                    )
             pair_copy(k, zq).start()
+            gain_mine[0, :, both] += gains
             return carry
 
         lax.fori_loop(0, nz, step, 0)
@@ -1009,6 +1025,14 @@
 
     factors = (1.0, 1.0, 0.5)
 
+    def put(k, m):
+        return pltpu.make_async_copy(
+            sums.at[m, hold(k), :], sum_outs[m].at[hold(k), :], sum_sem.at[k, m]
+        )
+
+    def put_tokens(a):
+        return pltpu.make_async_copy((early_raw, late_raw)[a], token_outs[1 - a], token_sem.at[a])
+
     def finish(k):
         pair_copy(k, z).wait_recv()
 
@@ -1031,7 +1055,8 @@
         @pl.when(straight)
         def _():
             for m in range(3):
-                sum_outs[m][hold(k), :] = sums[m, hold(k), :] + factors[m] * total(m)
+                sums[m, hold(k), :] += factors[m] * total(m)
+                put(k, m).start()
 
         @pl.when(x != c)
         def _():
@@ -1044,9 +1069,8 @@
         def _():
             back(k).wait_recv()
             for m in range(3):
-                sum_outs[m][hold(k), :] = sums[m, hold(k), :] + factors[m] * back_got[
-                    m, hold(k), :
-                ].astype(f32)
+                sums[m, hold(k), :] += factors[m] * back_got[m, hold(k), :].astype(f32)
+                put(k, m).start()
 
     low, high = (0, split), (split, tokens - split)
 
@@ -1076,14 +1100,6 @@
         ).astype(bf16)
         part[0, where, :] = both
 
-    def gain_half(side):
-        def step(i, total):
-            where = some(side * 2 * tokens + i * 16, 16)
-            term = part[0, where, :].astype(f32) * toks[0, where, :].astype(f32)
-            return total + term[:8] + term[8:]
-
-        return lax.fori_loop(0, tokens // 8, step, jnp.zeros((8, depth), f32))
-
     def late_half(side):
         where = half_of(side)
         part[1, where, :] = dot(hid_l[where, :], wall[2], ((1,), (0,))).astype(bf16)
@@ -1113,7 +1129,7 @@
     def write_late():
         def step(i, carry):
             where = some(i * 16, 16)
-            late_out[where, :] = (
+            late_raw[where, :] = (
                 late_raw[where, :].astype(f32) + 0.5 * own_total(1, i)
             ).astype(bf16)
             return carry
@@ -1125,10 +1141,10 @@
             where = some(i * 16, 16)
             values = early_raw[where, :].astype(f32)
             scale = lax.rsqrt(jnp.mean(values * values, axis=-1, keepdims=True) + epsilon)
-            scaled = own_total(0, i) * gain_ref[...]
+            scaled = own_total(0, i) * gain_f[...]
             mean = jnp.mean(values * scaled, axis=-1, keepdims=True)
             cot = toks[1, some(p_me * tokens + i * 16, 16), :].astype(f32)
-            early_out[where, :] = (cot + scale * scaled - values * scale**3 * mean).astype(bf16)
+            early_raw[where, :] = (cot + scale * scaled - values * scale**3 * mean).astype(bf16)
             return carry
 
         lax.fori_loop(0, tokens // 16, step, 0)
@@ -1162,20 +1178,68 @@
             for away in range(1, nz):
                 gain_away(away).start()
 
+    def each_step(steps):
+        for step in steps:
+            if step[1] == 0:
+                lead(step[0])
+                follow(step[0])
+            elif step[1] < 0:
+                (lead, follow)[step[1] + 2](step[0])
+            else:
+                pump(*step)
+
+    def when_straight(*steps):
+        @pl.when(straight)
+        def _():
+            each_step(steps)
+
+    def when_crossed(*steps):
+        @pl.when(x != c)
+        def _():
+            each_step(steps)
+
+    inner = (z > 0) & (z < nz - 1)
+
+    def when_inner(*steps):
+        @pl.when(inner)
+        def _():
+            each_step(steps)
+
+    def when_outer(*steps):
+        @pl.when(jnp.logical_not(inner))
+        def _():
+            each_step(steps)
+
+    gain_f[...] = gain_ref[...].astype(f32).reshape(1, depth)
+    loads[0].wait()
+    norm(early_raw, 0)
+
+    @pl.when(straight)
+    def _():
+        pl.semaphore_wait(barrier, nz - 1 + 3)
+
     @pl.when(x != c)
     def _():
-        for m in range(3):
-            swap(0, m).start()
-
-    tok(1, 0).start()
-    tok(1, 1).start()
-    loads[0].wait()
-    norm(early_raw, 0)
-    tok(0, 0).start()
-    tok(0, 1).start()
-    pump(0, 0)
+        pl.semaphore_wait(barrier, nz - 1 + 4)
+
+    @pl.when(x != c)
+    def _():
+        for k in range(count):
+            for m in range(3):
+                swap(k, m).start()
+
+    for a in range(2):
+        tok(a, 1).start()
+
+    @pl.when(x != c)
+    def _():
+        for a in range(2):
+            tok(a, 0).start()
+
+    when_straight((0, 0), (1, -2))
     loads[1].wait()
     norm(late_raw, 2)
+    gain_mine[0] = jnp.zeros((1, depth), f32)
 
     @pl.when(z == 0)
     def _():
@@ -1185,86 +1249,113 @@
     def _():
         slots[nz] = jnp.zeros_like(slots[nz])
 
-    tok_forward(1)
-    pump(0, 1)
-    tok_forward(0)
-
-    @pl.when(x != c)
+    when_crossed((0, 0))
+    when_straight((0, 1))
+
+    @pl.when(straight)
     def _():
-        for k in range(1, count):
-            for m in range(3):
-                swap(k, m).start()
-
+        for a in range(2):
+            tok(a, 0).start()
+
+    tok_over_x(0)
+    when_straight((2, -2), (0, 2), (1, -1))
+    when_crossed((1, -2), (0, 1))
+    tok_over_y(0)
+    when_straight((0, 3), (1, 1))
+    when_crossed((2, -2), (0, 2), (1, -1))
+    loads[2].wait()
+    tok_over_x(1)
+    tok_over_y(1)
+    tok_rest(0)
+    when_crossed((0, 3))
+    weights_in(0)
+    act_first(0)
+    when_straight((1, 2), (2, -1))
+    tok_rest(1)
+    tok(2, 1).start()
     tok(2, 0).start()
-    tok(2, 1).start()
-    for d in range(2, nz):
-        pump(0, d)
-    if count > 1:
-        pump(1, 0)
-    loads[2].wait()
-    tok_rest(1)
-    tok_rest(0)
-    for k in range(count):
-        weights_in(k)
-        act_early(k)
-        products(k)
-        combine_free(k)
-        if k == 0:
-            tok_forward(2)
-        if k < count - 1:
-            for d in range(1, nz):
-                pump(k + 1, d)
-                combine_up(k, d - 1)
-                if d == 1:
-                    if k == 0:
-                        tok_rest(2)
-                    act_late(k)
-            combine_up(k, nz - 1)
-            if k + 2 < count:
-                pump(k + 2, 0)
-    if count == 1:
-        tok_rest(2)
-    act_late(count - 1)
+    act_second(0)
+    products(0)
+    combine_free(0)
+    when_crossed((1, 1), (1, 2), (2, -1))
+    when_inner((2, 1))
+    when_outer((1, 3))
+    tok_over_x(2)
+    tok_over_y(2)
+    combine_up(0, 0)
+    when_inner((2, 2))
+    weights_in(1)
+    act_first(1)
+    act_second(1)
+    products(1)
+    combine_free(1)
+    combine_up(0, 1)
+    when_outer((2, 1), (2, 2), (2, 3))
+    tok_rest(2)
+    act_late(0)
+    combine_up(0, 2)
+    combine_up(0, 3)
+    act_late(1)
+    weights_in(2)
+    act_first(2)
+    act_second(2)
+    products(2)
+    gain_mine[0] = gain_mine[0] / gain_f[...]
+    gain_step(0).start()
     grad_half(1 - x)
+    gain_next(0)
     for kind in range(3):
         share(0, kind).start()
+    act_late(2)
+    gain_next(1)
     late_half(1 - x)
     for kind in range(3):
         share(1, kind).start()
+    combine_free(2)
+    combine_up(1, 0)
     grad_half(x)
     share(0, 3).start()
     late_half(x)
     share(1, 3).start()
-    gain = jnp.sum(gain_half(1 - x) + gain_half(x), axis=0, keepdims=True)
-    gain_mine[0] = gain / gain_ref[...]
-    gain_step(0).start()
+    gain_next(2)
+    combine_up(1, 1)
+    share_forward(0)
+    combine_up(1, 2)
+    combine_up(1, 3)
     for i in range(3):
         loads[3 + i].wait()
-    for k in range(count - 1):
-        finish(k)
-    combine_up(count - 1, 0)
-    share_forward(0)
-    gain_next(0)
-    combine_up(count - 1, 1)
+    finish(0)
+    combine_up(2, 0)
     share_forward(1)
-    gain_next(1)
-    for i in range(2, nz):
-        combine_up(count - 1, i)
-    gain_next(2)
+    combine_up(2, 1)
+    finish(1)
+    combine_up(2, 2)
+    combine_up(2, 3)
+    finish(2)
+    finish_back(0)
     share_in(0)
     write_early()
+    put_tokens(0).start()
     share_in(1)
     write_late()
+    put_tokens(1).start()
     for away in range(1, nz):
         gain_away(away).wait_recv()
     total = gain_z[0]
     for k in range(1, nz):
         total = total + gain_z[k]
-    gain_out[...] = gain_sum_ref[...] + total
-    finish(count - 1)
+    gain_got[2] = gain_sum_ref[...] + total
+    put_gain = pltpu.make_async_copy(gain_got.at[2], gain_out, gain_sem)
+    put_gain.start()
+    finish_back(1)
+    finish_back(2)
+
+    put_gain.wait()
+    for a in range(2):
+        put_tokens(a).wait()
     for k in range(count):
-        finish_back(k)
-
+        for m in range(3):
+            put(k, m).wait()
     for i in range(3):
         gain_step(i).wait_send()
     for away in range(1, nz):
@@ -1312,14 +1403,14 @@
     f32, bf16 = jnp.float32, jnp.bfloat16
     dma = pltpu.SemaphoreType.DMA
     crowd = 4 * tokens
-    split = tokens // 2
+    split = tokens * 3 // 128 * 16
     return pl.pallas_call(
         functools.partial(fused_kernel, n, cuts),
         out_shape=[jax.ShapeDtypeStruct((tokens, depth), bf16)] * 2
         + [jax.ShapeDtypeStruct((width, rows), f32)] * 3
         + [jax.ShapeDtypeStruct((1, depth), f32)],
         in_specs=[hbm] * 6 + [vmem] + [hbm] * 3 + [vmem],
-        out_specs=[vmem] * 6,
+        out_specs=[hbm] * 6,
         scratch_shapes=[
             pltpu.VMEM((3, width, depth), bf16),
             pltpu.VMEM((3, crowd, depth), bf16),
@@ -1364,6 +1455,10 @@
             dma((2, 6)),
             dma((2 + nz,)),
             dma((2 + nz,)),
+            dma((2,)),
+            dma((count, 3)),
+            dma(()),
+            pltpu.VMEM((1, depth), f32),
         ],
         compiler_params=pltpu.CompilerParams(
             collective_id=2, has_side_effects=True, vmem_limit_bytes=FUSED_LIMIT
@@ -1371,9 +1466,43 @@
     )(gate, up, dn, late, early, cot, gain, *sums, gain_sum)
 
 
+def settle_kernel(*refs):
+    count = len(refs) // 3
+    sources, targets, buffers = refs[:count], refs[count : 2 * count], refs[2 * count : 3 * count]
+    in_sem, out_sem = refs[3 * count :]
+    reads = [
+        pltpu.make_async_copy(source, buffer, in_sem.at[k])
+        for k, (source, buffer) in enumerate(zip(sources, buffers))
+    ]
+    writes = [
+        pltpu.make_async_copy(buffer, target, out_sem.at[k])
+        for k, (buffer, target) in enumerate(zip(buffers, targets))
+    ]
+    for copy in reads:
+        copy.start()
+    for read, write in zip(reads, writes):
+        read.wait()
+        write.start()
+    for copy in writes:
+        copy.wait()
+
+
+def settle(arrays):
+    hbm = pl.BlockSpec(memory_space=pl.ANY)
+    return pl.pallas_call(
+        settle_kernel,
+        out_shape=[jax.ShapeDtypeStruct(array.shape, array.dtype) for array in arrays],
+        in_specs=[hbm] * len(arrays),
+        out_specs=[hbm] * len(arrays),
+        scratch_shapes=[pltpu.VMEM(array.shape, array.dtype) for array in arrays]
+        + [pltpu.SemaphoreType.DMA((len(arrays),))] * 2,
+        compiler_params=pltpu.CompilerParams(vmem_limit_bytes=VMEM_LIMIT),
+    )(*arrays)
+
+
 def cut_hidden(width):
-    first = min(width, -(-width // 256) * 128)
-    return tuple(cut for cut in ((0, first), (first, width - first)) if cut[1])
+    step = -(-width // 384) * 128
+    return tuple((at, min(step, width - at)) for at in range(0, width, step))
 
 
 def per_device_fused(n, args):
@@ -1388,16 +1517,16 @@
         late,
         early,
         cot,
-        norm_gain.astype(jnp.float32).reshape(1, depth),
+        norm_gain,
         (gate_sum.T, up_sum.T, dn_sum.T),
         gain_sum.reshape(1, depth),
     )
-    late_out, early_grad, gate_out, up_out, dn_out, gain_out = out
+    late_out, early_grad, gate_out, up_out, dn_out, gain_out = settle(out)
     return late_out, early_grad, gate_out.T, up_out.T, dn_out.T, gain_out.reshape(depth)
 
 
 def per_device(n, n_tp, *args):
-    if n_tp == 4 and n % 2 == 0 and args[2].shape[0] % 128 == 0:
+    if n == 8 and n_tp == 4 and len(cut_hidden(args[2].shape[1])) == 3 and args[2].shape[0] % 128 == 0:
         return per_device_fused(n, args)
     return per_device_rings(n, n_tp, *args)
 

time: 174 us -> 147 us (0.84)
  Pallas kernels: 164 us -> 145 us
  local copies, waits for them, and re-layouts: 8.12 us -> 0 us
    pallas_call x1, Pallas kernels: 164 us -> 143 us  [fused(): pl.pallas_call(functools.partial(fused_kernel, n, cuts), out_shape=[jax.S...]
    unnamed x18 -> x0, local copies, waits for them, and re-layouts: 8.12 us -> none
    pallas_call x0 -> x1, Pallas kernels: none -> 2.87 us  [settle(): pl.pallas_call(settle_kernel, out_shape=[jax.ShapeDtypeStruct(array.shape...]
where the time goes in v2:
time: 147 us; the launch traced here: 146 us
  Pallas kernels  145 us (99%)
    pallas_call x1, Pallas kernels, fused(): pl.pallas_call(functools.partial(fused_kernel, n, cuts), out_shape=[jax.S...  143 us

profile of v2, /device:TPU:1, one launch (start us, length us, event | category | flops | bytes accessed | tf_op | source)
XLA Modules:
  0.0 146.3 jit_solution(7309597771368937518)
XLA Ops:
  0.6 142.6 %shard_map.154 = (bf16[128,2048]{1,0:T(8,128)(2,1)}, bf16[128,2048]{1,0:T(8,128)(2,1)}, f32[704,256]{1,0:T(8,128)}, f32[704,256]{1,0:T(8,128)}, f32[704,256]{1,0:T(8,128)}, /*index=5*/f32[1,2048]{1,0:T(1,128)}) custom-call(bf16[704,256]{1,0:T(8,128)(2,1)} %bitcast.14, bf16[704,256]{1,0:T(8,128)(2,1)} %bitcast.15, bf16[704,256]{1,0:T(8,128)(2,1)} %bitcast.16, ...), custom_call_target="tpu_custom_call" | custom-call | tf_op jit(solution)/shard_map/pallas_call | solution.py:1407
  143.2 2.9 %shard_map.155 = (bf16[128,2048]{1,0:T(8,128)(2,1)}, bf16[128,2048]{1,0:T(8,128)(2,1)}, f32[704,256]{1,0:T(8,128)}, f32[704,256]{1,0:T(8,128)}, f32[704,256]{1,0:T(8,128)}, /*index=5*/f32[1,2048]{1,0:T(1,128)}) custom-call(bf16[128,2048]{1,0:T(8,128)(2,1)} %get-tuple-element.18.refs_0_, bf16[128,2048]{1,0:T(8,128)(2,1)} %get-tuple-element.19.refs_1_, ...), custom_call_target="tpu_custom_call" | custom-call | tf_op jit(solution)/shard_map/pallas_call | solution.py:1492

commit v3 on v2

--- a/solution.py
+++ b/solution.py
@@ -672,8 +672,8 @@
     weights = (gate_in, up_in, dn_in)
     tokens, depth = late_in.shape
     width, rows = gate_in.shape
-    split = tokens * 3 // 128 * 16
-    tok_splits = (16, split, tokens // 2)
+    split = tokens // 64 * 16
+    tok_splits = (16, tokens // 2, tokens // 2)
     bf16, f32 = jnp.bfloat16, jnp.float32
     count = len(cuts)
     straight = x == c
@@ -983,11 +983,12 @@
     def upstream(zq):
         return ((zq > z) & (z > 0)) | ((zq < z) & (z < nz - 1))
 
-    def combine_free(k):
+    def combine_free(k, least=1, most=nz):
         def step(i, carry):
             zq = turn(i)
-
-            @pl.when((zq != z) & jnp.logical_not(upstream(zq)))
+            away = jnp.abs(zq - z)
+
+            @pl.when((away >= least) & (away <= most) & jnp.logical_not(upstream(zq)))
             def _():
                 pair_copy(k, zq).wait_recv()
                 for m in range(3):
@@ -1200,6 +1201,16 @@
 
     inner = (z > 0) & (z < nz - 1)
 
+    def when_straight_inner(*steps):
+        @pl.when(straight & inner)
+        def _():
+            each_step(steps)
+
+    def when_straight_outer(*steps):
+        @pl.when(straight & jnp.logical_not(inner))
+        def _():
+            each_step(steps)
+
     def when_inner(*steps):
         @pl.when(inner)
         def _():
@@ -1224,7 +1235,7 @@
 
     @pl.when(x != c)
     def _():
-        for k in range(count):
+        for k in range(2):
             for m in range(3):
                 swap(k, m).start()
 
@@ -1262,21 +1273,39 @@
     when_crossed((1, -2), (0, 1))
     tok_over_y(0)
     when_straight((0, 3), (1, 1))
-    when_crossed((2, -2), (0, 2), (1, -1))
+    when_crossed((0, 2), (1, -1))
     loads[2].wait()
     tok_over_x(1)
+
+    @pl.when(x != c)
+    def _():
+        for m in range(3):
+            swap(2, m).start()
+
     tok_over_y(1)
     tok_rest(0)
     when_crossed((0, 3))
     weights_in(0)
     act_first(0)
-    when_straight((1, 2), (2, -1))
+    when_straight_inner((1, 2), (2, -1))
     tok_rest(1)
-    tok(2, 1).start()
-    tok(2, 0).start()
+
+    @pl.when(straight)
+    def _():
+        tok(2, 1).start()
+        tok(2, 0).start()
+
     act_second(0)
     products(0)
+    when_crossed((2, -2))
     combine_free(0)
+
+    @pl.when(x != c)
+    def _():
+        tok(2, 1).start()
+        tok(2, 0).start()
+
+    when_straight_outer((1, 2), (2, -1))
     when_crossed((1, 1), (1, 2), (2, -1))
     when_inner((2, 1))
     when_outer((1, 3))
@@ -1288,14 +1317,16 @@
     act_first(1)
     act_second(1)
     products(1)
-    combine_free(1)
+    combine_free(1, 2)
     combine_up(0, 1)
-    when_outer((2, 1), (2, 2), (2, 3))
+    when_outer((2, 1))
     tok_rest(2)
     act_late(0)
+    when_outer((2, 2))
+    act_late(1)
     combine_up(0, 2)
     combine_up(0, 3)
-    act_late(1)
+    when_outer((2, 3))
     weights_in(2)
     act_first(2)
     act_second(2)
@@ -1306,31 +1337,31 @@
     gain_next(0)
     for kind in range(3):
         share(0, kind).start()
+    combine_free(2, 2)
+    combine_free(1, 1, 1)
+    combine_free(2, 1, 1)
     act_late(2)
+    late_half(1 - x)
     gain_next(1)
-    late_half(1 - x)
     for kind in range(3):
         share(1, kind).start()
-    combine_free(2)
+    for i in range(3):
+        loads[3 + i].wait()
+    finish(0)
     combine_up(1, 0)
     grad_half(x)
     share(0, 3).start()
     late_half(x)
     share(1, 3).start()
+    combine_up(1, 1)
+    combine_up(1, 2)
+    share_forward(0)
+    combine_up(2, 0)
     gain_next(2)
-    combine_up(1, 1)
-    share_forward(0)
-    combine_up(1, 2)
-    combine_up(1, 3)
-    for i in range(3):
-        loads[3 + i].wait()
-    finish(0)
-    combine_up(2, 0)
+    combine_up(2, 2)
     share_forward(1)
     combine_up(2, 1)
     finish(1)
-    combine_up(2, 2)
-    combine_up(2, 3)
     finish(2)
     finish_back(0)
     share_in(0)
@@ -1403,7 +1434,7 @@
     f32, bf16 = jnp.float32, jnp.bfloat16
     dma = pltpu.SemaphoreType.DMA
     crowd = 4 * tokens
-    split = tokens * 3 // 128 * 16
+    split = tokens // 64 * 16
     return pl.pallas_call(
         functools.partial(fused_kernel, n, cuts),
         out_shape=[jax.ShapeDtypeStruct((tokens, depth), bf16)] * 2

time: 147 us -> 142 us (0.966)
  Pallas kernels: 145 us -> 141 us
    pallas_call x1, Pallas kernels: 143 us -> 138 us  [fused(): pl.pallas_call(functools.partial(fused_kernel, n, cuts), out_shape=[jax.S...]
where the time goes in v3:
time: 142 us; the launch traced here: 141 us
  Pallas kernels  141 us (99%)
    pallas_call x1, Pallas kernels, fused(): pl.pallas_call(functools.partial(fused_kernel, n, cuts), out_shape=[jax.S...  138 us
    pallas_call x1, Pallas kernels, settle(): pl.pallas_call(settle_kernel, out_shape=[jax.ShapeDtypeStruct(array.shape...  2.87 us

profile of v3, /device:TPU:1, one launch (start us, length us, event | category | flops | bytes accessed | tf_op | source)
XLA Modules:
  0.0 141.4 jit_solution(12988556320652130242)
XLA Ops:
  0.6 137.7 %shard_map.154 = (bf16[128,2048]{1,0:T(8,128)(2,1)}, bf16[128,2048]{1,0:T(8,128)(2,1)}, f32[704,256]{1,0:T(8,128)}, f32[704,256]{1,0:T(8,128)}, f32[704,256]{1,0:T(8,128)}, /*index=5*/f32[1,2048]{1,0:T(1,128)}) custom-call(bf16[704,256]{1,0:T(8,128)(2,1)} %bitcast.14, bf16[704,256]{1,0:T(8,128)(2,1)} %bitcast.15, bf16[704,256]{1,0:T(8,128)(2,1)} %bitcast.16, ...), custom_call_target="tpu_custom_call" | custom-call | tf_op jit(solution)/shard_map/pallas_call | solution.py:1438
  138.4 2.9 %shard_map.155 = (bf16[128,2048]{1,0:T(8,128)(2,1)}, bf16[128,2048]{1,0:T(8,128)(2,1)}, f32[704,256]{1,0:T(8,128)}, f32[704,256]{1,0:T(8,128)}, f32[704,256]{1,0:T(8,128)}, /*index=5*/f32[1,2048]{1,0:T(1,128)}) custom-call(bf16[128,2048]{1,0:T(8,128)(2,1)} %get-tuple-element.18.refs_0_, bf16[128,2048]{1,0:T(8,128)(2,1)} %get-tuple-element.19.refs_1_, ...), custom_call_target="tpu_custom_call" | custom-call | tf_op jit(solution)/shard_map/pallas_call | solution.py:1523
